TPU v7x, 256 devices: a whole 4x4x8 slice. The times are simulated.
256 devices in a mesh: ep: 16 (over y, x), tp: 16 (over z, core).
Axes of the slice: x: 4, y: 4, z: 8, core: 2. Of those that a mesh axis runs over, the one named last changes fastest.
Arguments:
- queries: bfloat16 [16384, 1024], P('ep', 'tp'), may hold values from -8 to 8
- keys: bfloat16 [16384, 256], P('ep'), may hold values from -8 to 8
- values: bfloat16 [16384, 256], P('ep'), may hold values from -6 to 6
- query_gain: float32 [64], replicated, may hold values from 1 to 10
- key_gain: float32 [64], replicated, may hold values from 1 to 10
- moe_input: bfloat16 [12288, 2048], P(('ep', 'tp')), may hold values from -6 to 6
- expert_ids: int32 [12288, 2], P('ep'), may hold values from 0 to 15, all different within a row; in each aligned block of 48 rows (0 to 47, 48 to 95, ...) at most 7 rows name the same one
- route_weight: float32 [12288, 2], P('ep'), may hold values from 0.2 to 1
- gate_weight: bfloat16 [16, 2048, 7168], P('ep', None, 'tp'), may hold values from -0.125 to 0.125
- up_weight: bfloat16 [16, 2048, 7168], P('ep', None, 'tp'), may hold values from -0.125 to 0.125
- down_weight: bfloat16 [16, 7168, 2048], P('ep', 'tp'), may hold values from -0.0625 to 0.0625
- output_gain: float32 [2048], replicated, may hold values from 0.1 to 1.9
Outputs:
- attended: bfloat16 [16384, 1024], P('ep', 'tp')
- moe_output: bfloat16 [12288, 2048], P(('ep', 'tp'))
Inputs may be any that keep to these rules, and one draw needn't show every extreme that they name: `expert_ids`: the 2 experts of a token differ. In the rows of one device (aligned blocks of 48 tokens) no expert is named by more than 7 tokens, and in every draw some expert is named by exactly 7 tokens of some device.
All inputs are finite; a program needn't handle non-finite values.
Results may differ from a plain program's by a relative error of at most 0.0085.
The roundings to bfloat16 on the way count: a program that leaves them out, or rounds other values in their place, can miss the bound.
Values may be sent and summed in bfloat16 or wider, within the bound.
No kernel may reach another device: no remote copies, remote signals or barrier semaphores. Data moves between devices by JAX's collectives and lax.ppermute only.
A program may use at most 128 MiB of HBM per device.

v0:
```python
import math

import jax
import jax.numpy as jnp
from jax import lax
from jax.sharding import Mesh
from jax.sharding import PartitionSpec as P

QH = 16
KV = 4
GRID_W = 64
TP = ("tp_0", "tp_1")
EP_TP = ("ep", "tp_0", "tp_1")


rope_theta = 10000.0
rms_epsilon = 1e-06
norm_epsilon = 1e-05
residual_scale = 1.4142135623730951


def side_by_side(arrays, axis, dim, along):
    ends, at = ([], 0)
    for a in arrays[:-1]:
        at += a.shape[along]
        ends.append(at)
    both = jnp.concatenate(arrays, axis=along)
    return tuple(jnp.split(lax.all_gather(both, axis, axis=dim, tiled=True), ends, axis=along))


def sum_by_axis(terms, axes):
    subtotal = terms.astype(jnp.bfloat16)
    for axis in axes:
        subtotal = lax.psum_scatter(subtotal, axis, scatter_dimension=0, tiled=True)
    return subtotal.astype(jnp.float32)


def unit_heads(heads, gain_vector):
    squares = jnp.mean(heads * heads, axis=-1, keepdims=True)
    return heads * lax.rsqrt(squares + rms_epsilon) * gain_vector


def rotate_grid(heads, first_position, grid_width):
    head_size = heads.shape[-1]
    pair_count = head_size // 4
    position = first_position + jnp.arange(heads.shape[1], dtype=jnp.int32)
    grid_row = (position // grid_width).astype(jnp.float32)
    grid_col = (position % grid_width).astype(jnp.float32)
    inverse = rope_theta ** (-jnp.arange(pair_count, dtype=jnp.float32) / pair_count)
    angles = jnp.concatenate([grid_row[:, None] * inverse, grid_col[:, None] * inverse], axis=-1)
    cosines = jnp.cos(angles)
    sines = jnp.sin(angles)
    half_size = head_size // 2
    first_half = heads[..., :half_size]
    second_half = heads[..., half_size:]
    return jnp.concatenate(
        [first_half * cosines - second_half * sines, second_half * cosines + first_half * sines],
        axis=-1,
    )


def place_rank(choices, expert_count):
    matches = (choices[..., None] == jnp.arange(expert_count, dtype=jnp.int32)).astype(jnp.int32)
    earlier = jnp.cumsum(matches, axis=1) - matches
    return jnp.sum(earlier * matches, axis=-1)


def shards(
    queries,
    keys,
    values,
    query_gain,
    key_gain,
    moe_input,
    expert_ids,
    route_weight,
    gate_weight,
    up_weight,
    down_weight,
    output_gain,
):
    seg_rows = queries.shape[0]
    head_size = query_gain.shape[0]
    local_heads = queries.shape[1] // head_size
    offset = lax.axis_index("ep") * seg_rows
    key_head = lax.axis_index(TP) * local_heads // (QH // KV)
    key_cols = lax.dynamic_slice_in_dim(keys, key_head * head_size, head_size, 1)
    value_cols = lax.dynamic_slice_in_dim(values, key_head * head_size, head_size, 1)
    query_heads = (
        queries.reshape(seg_rows, local_heads, head_size).transpose(1, 0, 2).astype(jnp.float32)
    )
    rotated_queries = rotate_grid(unit_heads(query_heads, query_gain), offset, GRID_W).astype(
        jnp.bfloat16
    )
    key_heads = key_cols.astype(jnp.float32)[None]
    rotated_keys = rotate_grid(unit_heads(key_heads, key_gain), offset, GRID_W)[0].astype(
        jnp.bfloat16
    )
    score_scale = head_size ** (-0.5)
    initial = (
        jnp.full((local_heads, seg_rows), -jnp.inf, jnp.float32),
        jnp.zeros((local_heads, seg_rows), jnp.float32),
        jnp.zeros((local_heads, head_size, seg_rows), jnp.float32),
    )
    key_piece, value_piece = side_by_side((rotated_keys, value_cols), "ep", 0, 1)
    piece_rows = key_piece.shape[0]
    block_rows = math.gcd(piece_rows, 1024)
    key_blocks = key_piece.reshape(piece_rows // block_rows, block_rows, head_size)
    value_blocks = value_piece.reshape(piece_rows // block_rows, block_rows, head_size)

    def sweep(state_now, blocks):
        running_max, row_total, summed = state_now
        key_block, value_block = blocks
        scores = (
            jnp.einsum(
                "hqd,kd->hqk", rotated_queries, key_block, preferred_element_type=jnp.float32
            )
            * score_scale
        )
        new_max = jnp.maximum(running_max, jnp.max(scores, axis=-1))
        shrink = jnp.exp(running_max - new_max)
        weights = jnp.exp(scores - new_max[..., None])
        row_total = row_total * shrink + jnp.sum(weights, axis=-1)
        added = jnp.einsum(
            "hqk,kd->hdq",
            weights.astype(jnp.bfloat16),
            value_block,
            preferred_element_type=jnp.float32,
        )
        summed = summed * shrink[:, None, :] + added
        return ((new_max, row_total, summed), None)

    result, ignored = lax.scan(sweep, initial, (key_blocks, value_blocks))
    row_max, row_total, summed = result
    attended = (
        (summed / row_total[:, None, :])
        .transpose(2, 0, 1)
        .reshape(seg_rows, local_heads * head_size)
        .astype(jnp.bfloat16)
    )
    tok_rows = moe_input.shape[0]
    model_width = moe_input.shape[1]
    top_count = expert_ids.shape[1]
    experts = lax.axis_size("ep")
    capacity = max(2, tok_rows * top_count * 5 // (4 * experts))
    column_index = lax.axis_index(TP)
    own_ids = lax.dynamic_slice_in_dim(expert_ids, column_index * tok_rows, tok_rows, 0).reshape(-1)
    own_weights = lax.dynamic_slice_in_dim(route_weight, column_index * tok_rows, tok_rows, 0)
    own_rank = place_rank(own_ids[None], experts)[0]
    own_slots = own_ids * capacity + own_rank
    token_of = jnp.arange(tok_rows * top_count, dtype=jnp.int32) // top_count
    sources = jnp.full((experts * capacity,), tok_rows, jnp.int32).at[own_slots].set(token_of)
    outgoing = jnp.take(moe_input, sources, axis=0, mode="fill", fill_value=0)
    arrived = lax.all_to_all(
        outgoing.reshape(experts, capacity, model_width),
        "ep",
        split_axis=0,
        concat_axis=0,
        tiled=True,
    )
    shard_piece = lax.all_gather(arrived.reshape(-1, model_width), TP, axis=0, tiled=True)
    gate_part = jnp.dot(shard_piece, gate_weight[0], preferred_element_type=jnp.float32)
    up_part = jnp.dot(shard_piece, up_weight[0], preferred_element_type=jnp.float32)
    hidden = (jax.nn.silu(gate_part) * up_part).astype(jnp.bfloat16)
    expert_out = sum_by_axis(
        jnp.dot(hidden, down_weight[0], preferred_element_type=jnp.float32), TP
    ).astype(jnp.bfloat16)
    returned = lax.all_to_all(
        expert_out.reshape(experts, capacity, model_width),
        "ep",
        split_axis=0,
        concat_axis=0,
        tiled=True,
    )
    picked = jnp.take(returned.reshape(experts * capacity, model_width), own_slots, axis=0)
    picked = picked.reshape(tok_rows, top_count, model_width).astype(jnp.float32)
    mixed = residual_scale * moe_input.astype(jnp.float32) + jnp.sum(
        own_weights[:, :, None] * picked, axis=1
    )
    average = jnp.mean(mixed, axis=-1, keepdims=True)
    centered = mixed - average
    variance = jnp.mean(centered * centered, axis=-1, keepdims=True)
    moe_output = (centered * lax.rsqrt(variance + norm_epsilon) * output_gain).astype(jnp.bfloat16)
    return (attended, moe_output)


def solution(mesh):
    split = Mesh(mesh.devices.reshape(mesh.shape["ep"], 8, 2), ("ep", "tp_0", "tp_1"))
    return jax.shard_map(
        shards,
        mesh=split,
        in_specs=(
            P("ep", TP),
            P("ep", None),
            P("ep", None),
            P(),
            P(),
            P(EP_TP, None),
            P("ep", None),
            P("ep", None),
            P("ep", None, TP),
            P("ep", None, TP),
            P("ep", TP, None),
            P(),
        ),
        out_specs=(P("ep", TP), P(EP_TP, None)),
        check_vma=False,
    )
```

profile of v0, /device:TPU:4, one launch (start us, length us, event | category | flops | bytes accessed | tf_op | source)
XLA Modules:
  0.0 364.8 jit_solution(13836861877901142481)
XLA Ops:
  10.7 2.3 gather_fusion
  13.4 16.2 %all_to_all.10 = bf16[16,7,2048]{2,1,0:T(8,128)(2,1)S(1)} all-to-all(bf16[16,7,2048]{2,1,0:T(8,128)(2,1)S(1)} %broadcast_select_fusion.3), channel_id=1, replica_groups=mesh['ep'=16,'tp_0'=8,'tp_1'=2] {'ep'}, dimensions={0} | all-to-all | bytes 917504 | tf_op jit(solution)/shard_map/all_to_all | solution.py:154
  30.5 52.3 %all-gather.5.cloned.1.call-done = bf16[1792,2048]{1,0:T(8,128)(2,1)} async-done(((bf16[112,2048]{1,0:T(8,128)(2,1)}), bf16[1792,2048]{1,0:T(8,128)(2,1)}) %all-gather.5.cloned.1.call-update) | async-done | bytes 7340048 | tf_op jit(solution)/shard_map/all_gather | solution.py:161
  82.8 7.3 %fusion.24 = f32[1792,448]{0,1:T(8,128)S(1)} fusion(bf16[1792,2048]{1,0:T(8,128)(2,1)} %all-gather.5.cloned.1.call-done, bf16[1,2048,448]{1,2,0:T(8,128)(2,1)} %param.22), kind=kOutput, calls=%fused_computation.30 | convolution fusion | flops 3288334336 | bytes 12386304 | tf_op jit(solution)/shard_map/dot_general | solution.py:162
  90.1 3.8 %multiply_convert_fusion = bf16[1792,448]{0,1:T(8,128)(2,1)S(1)} fusion(f32[1792,448]{0,1:T(8,128)S(1)} %fusion.24, bf16[1792,2048]{1,0:T(8,128)(2,1)S(1)} %copy-done.8, bf16[1,2048,448]{1,2,0:T(8,128)(2,1)S(1)} %copy-done.9), kind=kOutput, calls=%fused_computation.27 | convolution fusion | flops 3293151232 | bytes 13991936 | tf_op jit(solution)/shard_map/dot_general | solution.py:163
  93.9 6.1 %convolution_convert_fusion = bf16[1792,2048]{1,0:T(8,128)(2,1)} fusion(bf16[1792,448]{0,1:T(8,128)(2,1)S(1)} %multiply_convert_fusion, bf16[1,448,2048]{2,1,0:T(8,128)(2,1)S(1)} %copy-done), kind=kOutput, calls=%fused_computation.26 | convolution fusion | flops 3292004352 | bytes 10780672 | tf_op jit(solution)/shard_map/dot_general | solution.py:166
  105.9 77.9 %reduce-scatter.3.cloned.1.call-done = bf16[224,2048]{1,0:T(8,128)(2,1)} async-done(((bf16[1792,2048]{1,0:T(8,128)(2,1)}), bf16[224,2048]{1,0:T(8,128)(2,1)}) %reduce-scatter.3.cloned.1.call-update) | async-done | bytes 917520 | tf_op jit(solution)/shard_map/reduce_scatter | solution.py:34
  183.9 4.7 %fusion.47 = (bf16[16384,64]{0,1:T(8,128)(2,1)}, bf16[16384,64]{0,1:T(8,128)(2,1)}) fusion(bf16[16384,128]{0,1:T(8,128)(2,1)} %all-gather.3.cloned.1.call-done), kind=kLoop, calls=%fused_computation.105 | loop fusion | bytes 8388608 | tf_op jit(solution)/shard_map/split | solution.py:28
  188.5 4.8 %copy.37 = bf16[16384,64]{1,0:T(8,128)(2,1)} copy(bf16[16384,64]{0,1:T(8,128)(2,1)} %get-tuple-element.101) | data formatting | bytes 4194304
  193.3 5.0 %copy.38 = bf16[16384,64]{1,0:T(8,128)(2,1)} copy(bf16[16384,64]{0,1:T(8,128)(2,1)} %get-tuple-element.100) | data formatting | bytes 4194304
  198.6 2.0 reshape.467
  200.5 7.3 %all-to-all-start.1 = ((bf16[16,7,2048]{2,1,0:T(8,128)(2,1)}), bf16[16,7,2048]{2,1,0:T(8,128)(2,1)S(1)}, u32[]{:S(2)}, u32[]{:S(2)}) async-start(bf16[16,7,2048]{2,1,0:T(8,128)(2,1)} %reshape.467), calls=%async_computation.3 | async-start | bytes 1048576 | tf_op jit(solution)/shard_map/all_to_all | solution.py:168
  207.8 144.6 %while.15 = (s32[]{:T(128)}, f32[1,1024]{1,0:T(1,128)S(1)}, f32[1,1024]{1,0:T(1,128)S(1)}, f32[1,64,1024]{2,1,0:T(8,128)S(1)}, bf16[16,1024,64]{2,1,0:T(8,128)(2...) while((s32[]{:T(128)}, f32[1,1024]{1,0:T(1,128)S(1)}, ...), condition=%wide.region_5.6_spmd.clone, body=%wide.region_2.5_spmd.clone.sunk | while | flops 277025792 | bytes 30605460 | solution.py:133
  207.8 3.8 %multiply_reduce_fusion.4 = (f32[1024]{0:T(1024)S(1)}, f32[1024,1024]{1,0:T(8,128)}) fusion(bf16[1,1024,64]{2,1,0:T(8,128)(2,1)S(1)} %get-tuple-element.188, bf16[16,1024,64]{2,1,0:T(8,128)(2,1)} %get-tuple-element.187, s32[]{:T(128)S(6)} %copy.45), kind=kOutput, calls=%fused_computation.4.clone.1 | convolution fusion | flops 136313856 | bytes 4591620 | tf_op jit(solution)/shard_map/while/body/eval_jaxpr/hqd,kd->hqk/dot_general | solution.py:115
  211.6 3.1 fusion.60
  215.0 1.8 fusion.62
  216.8 3.8 %multiply_reduce_fusion.4 = (f32[1024]{0:T(1024)S(1)}, f32[1024,1024]{1,0:T(8,128)}) fusion(bf16[1,1024,64]{2,1,0:T(8,128)(2,1)S(1)} %get-tuple-element.188, bf16[16,1024,64]{2,1,0:T(8,128)(2,1)} %get-tuple-element.187, s32[]{:T(128)S(6)} %copy.45), kind=kOutput, calls=%fused_computation.4.clone.1 | convolution fusion | flops 136313856 | bytes 4591620 | tf_op jit(solution)/shard_map/while/body/eval_jaxpr/hqd,kd->hqk/dot_general | solution.py:115
  220.6 3.1 fusion.60
  225.9 3.8 %multiply_reduce_fusion.4 = (f32[1024]{0:T(1024)S(1)}, f32[1024,1024]{1,0:T(8,128)}) fusion(bf16[1,1024,64]{2,1,0:T(8,128)(2,1)S(1)} %get-tuple-element.188, bf16[16,1024,64]{2,1,0:T(8,128)(2,1)} %get-tuple-element.187, s32[]{:T(128)S(6)} %copy.45), kind=kOutput, calls=%fused_computation.4.clone.1 | convolution fusion | flops 136313856 | bytes 4591620 | tf_op jit(solution)/shard_map/while/body/eval_jaxpr/hqd,kd->hqk/dot_general | solution.py:115
  229.7 3.1 fusion.60
  233.1 1.8 fusion.62
  234.9 3.8 %multiply_reduce_fusion.4 = (f32[1024]{0:T(1024)S(1)}, f32[1024,1024]{1,0:T(8,128)}) fusion(bf16[1,1024,64]{2,1,0:T(8,128)(2,1)S(1)} %get-tuple-element.188, bf16[16,1024,64]{2,1,0:T(8,128)(2,1)} %get-tuple-element.187, s32[]{:T(128)S(6)} %copy.45), kind=kOutput, calls=%fused_computation.4.clone.1 | convolution fusion | flops 136313856 | bytes 4591620 | tf_op jit(solution)/shard_map/while/body/eval_jaxpr/hqd,kd->hqk/dot_general | solution.py:115
  238.7 3.1 fusion.60
  243.9 3.8 %multiply_reduce_fusion.4 = (f32[1024]{0:T(1024)S(1)}, f32[1024,1024]{1,0:T(8,128)}) fusion(bf16[1,1024,64]{2,1,0:T(8,128)(2,1)S(1)} %get-tuple-element.188, bf16[16,1024,64]{2,1,0:T(8,128)(2,1)} %get-tuple-element.187, s32[]{:T(128)S(6)} %copy.45), kind=kOutput, calls=%fused_computation.4.clone.1 | convolution fusion | flops 136313856 | bytes 4591620 | tf_op jit(solution)/shard_map/while/body/eval_jaxpr/hqd,kd->hqk/dot_general | solution.py:115
  247.7 3.1 fusion.60
  253.0 3.8 %multiply_reduce_fusion.4 = (f32[1024]{0:T(1024)S(1)}, f32[1024,1024]{1,0:T(8,128)}) fusion(bf16[1,1024,64]{2,1,0:T(8,128)(2,1)S(1)} %get-tuple-element.188, bf16[16,1024,64]{2,1,0:T(8,128)(2,1)} %get-tuple-element.187, s32[]{:T(128)S(6)} %copy.45), kind=kOutput, calls=%fused_computation.4.clone.1 | convolution fusion | flops 136313856 | bytes 4591620 | tf_op jit(solution)/shard_map/while/body/eval_jaxpr/hqd,kd->hqk/dot_general | solution.py:115
  256.8 3.1 fusion.60
  262.0 3.8 %multiply_reduce_fusion.4 = (f32[1024]{0:T(1024)S(1)}, f32[1024,1024]{1,0:T(8,128)}) fusion(bf16[1,1024,64]{2,1,0:T(8,128)(2,1)S(1)} %get-tuple-element.188, bf16[16,1024,64]{2,1,0:T(8,128)(2,1)} %get-tuple-element.187, s32[]{:T(128)S(6)} %copy.45), kind=kOutput, calls=%fused_computation.4.clone.1 | convolution fusion | flops 136313856 | bytes 4591620 | tf_op jit(solution)/shard_map/while/body/eval_jaxpr/hqd,kd->hqk/dot_general | solution.py:115
  265.8 3.1 fusion.60
  271.1 3.8 %multiply_reduce_fusion.4 = (f32[1024]{0:T(1024)S(1)}, f32[1024,1024]{1,0:T(8,128)}) fusion(bf16[1,1024,64]{2,1,0:T(8,128)(2,1)S(1)} %get-tuple-element.188, bf16[16,1024,64]{2,1,0:T(8,128)(2,1)} %get-tuple-element.187, s32[]{:T(128)S(6)} %copy.45), kind=kOutput, calls=%fused_computation.4.clone.1 | convolution fusion | flops 136313856 | bytes 4591620 | tf_op jit(solution)/shard_map/while/body/eval_jaxpr/hqd,kd->hqk/dot_general | solution.py:115
  274.8 3.1 fusion.60
  280.1 3.8 %multiply_reduce_fusion.4 = (f32[1024]{0:T(1024)S(1)}, f32[1024,1024]{1,0:T(8,128)}) fusion(bf16[1,1024,64]{2,1,0:T(8,128)(2,1)S(1)} %get-tuple-element.188, bf16[16,1024,64]{2,1,0:T(8,128)(2,1)} %get-tuple-element.187, s32[]{:T(128)S(6)} %copy.45), kind=kOutput, calls=%fused_computation.4.clone.1 | convolution fusion | flops 136313856 | bytes 4591620 | tf_op jit(solution)/shard_map/while/body/eval_jaxpr/hqd,kd->hqk/dot_general | solution.py:115
  283.9 3.1 fusion.60
  289.1 3.8 %multiply_reduce_fusion.4 = (f32[1024]{0:T(1024)S(1)}, f32[1024,1024]{1,0:T(8,128)}) fusion(bf16[1,1024,64]{2,1,0:T(8,128)(2,1)S(1)} %get-tuple-element.188, bf16[16,1024,64]{2,1,0:T(8,128)(2,1)} %get-tuple-element.187, s32[]{:T(128)S(6)} %copy.45), kind=kOutput, calls=%fused_computation.4.clone.1 | convolution fusion | flops 136313856 | bytes 4591620 | tf_op jit(solution)/shard_map/while/body/eval_jaxpr/hqd,kd->hqk/dot_general | solution.py:115
  292.9 3.1 fusion.60
  298.2 3.8 %multiply_reduce_fusion.4 = (f32[1024]{0:T(1024)S(1)}, f32[1024,1024]{1,0:T(8,128)}) fusion(bf16[1,1024,64]{2,1,0:T(8,128)(2,1)S(1)} %get-tuple-element.188, bf16[16,1024,64]{2,1,0:T(8,128)(2,1)} %get-tuple-element.187, s32[]{:T(128)S(6)} %copy.45), kind=kOutput, calls=%fused_computation.4.clone.1 | convolution fusion | flops 136313856 | bytes 4591620 | tf_op jit(solution)/shard_map/while/body/eval_jaxpr/hqd,kd->hqk/dot_general | solution.py:115
  301.9 3.1 fusion.60
  307.2 3.8 %multiply_reduce_fusion.4 = (f32[1024]{0:T(1024)S(1)}, f32[1024,1024]{1,0:T(8,128)}) fusion(bf16[1,1024,64]{2,1,0:T(8,128)(2,1)S(1)} %get-tuple-element.188, bf16[16,1024,64]{2,1,0:T(8,128)(2,1)} %get-tuple-element.187, s32[]{:T(128)S(6)} %copy.45), kind=kOutput, calls=%fused_computation.4.clone.1 | convolution fusion | flops 136313856 | bytes 4591620 | tf_op jit(solution)/shard_map/while/body/eval_jaxpr/hqd,kd->hqk/dot_general | solution.py:115
  311.0 3.1 fusion.60
  316.2 3.8 %multiply_reduce_fusion.4 = (f32[1024]{0:T(1024)S(1)}, f32[1024,1024]{1,0:T(8,128)}) fusion(bf16[1,1024,64]{2,1,0:T(8,128)(2,1)S(1)} %get-tuple-element.188, bf16[16,1024,64]{2,1,0:T(8,128)(2,1)} %get-tuple-element.187, s32[]{:T(128)S(6)} %copy.45), kind=kOutput, calls=%fused_computation.4.clone.1 | convolution fusion | flops 136313856 | bytes 4591620 | tf_op jit(solution)/shard_map/while/body/eval_jaxpr/hqd,kd->hqk/dot_general | solution.py:115
  320.0 3.1 fusion.60
  325.3 3.8 %multiply_reduce_fusion.4 = (f32[1024]{0:T(1024)S(1)}, f32[1024,1024]{1,0:T(8,128)}) fusion(bf16[1,1024,64]{2,1,0:T(8,128)(2,1)S(1)} %get-tuple-element.188, bf16[16,1024,64]{2,1,0:T(8,128)(2,1)} %get-tuple-element.187, s32[]{:T(128)S(6)} %copy.45), kind=kOutput, calls=%fused_computation.4.clone.1 | convolution fusion | flops 136313856 | bytes 4591620 | tf_op jit(solution)/shard_map/while/body/eval_jaxpr/hqd,kd->hqk/dot_general | solution.py:115
  329.1 3.1 fusion.60
  334.3 3.8 %multiply_reduce_fusion.4 = (f32[1024]{0:T(1024)S(1)}, f32[1024,1024]{1,0:T(8,128)}) fusion(bf16[1,1024,64]{2,1,0:T(8,128)(2,1)S(1)} %get-tuple-element.188, bf16[16,1024,64]{2,1,0:T(8,128)(2,1)} %get-tuple-element.187, s32[]{:T(128)S(6)} %copy.45), kind=kOutput, calls=%fused_computation.4.clone.1 | convolution fusion | flops 136313856 | bytes 4591620 | tf_op jit(solution)/shard_map/while/body/eval_jaxpr/hqd,kd->hqk/dot_general | solution.py:115
  338.1 3.1 fusion.60
  343.3 3.8 %multiply_reduce_fusion.4 = (f32[1024]{0:T(1024)S(1)}, f32[1024,1024]{1,0:T(8,128)}) fusion(bf16[1,1024,64]{2,1,0:T(8,128)(2,1)S(1)} %get-tuple-element.188, bf16[16,1024,64]{2,1,0:T(8,128)(2,1)} %get-tuple-element.187, s32[]{:T(128)S(6)} %copy.45), kind=kOutput, calls=%fused_computation.4.clone.1 | convolution fusion | flops 136313856 | bytes 4591620 | tf_op jit(solution)/shard_map/while/body/eval_jaxpr/hqd,kd->hqk/dot_general | solution.py:115
  347.1 3.1 fusion.60
  354.4 2.0 multiply_reduce_fusion.1
  (177 shorter events, 44.2 us)
Async XLA Ops:
  8.0 85.9 %copy-start = (bf16[1,448,2048]{2,1,0:T(8,128)(2,1)S(1)}, bf16[1,448,2048]{2,1,0:T(8,128)(2,1)}, u32[]{:S(2)}) copy-start(bf16[1,448,2048]{2,1,0:T(8,128)(2,1)} %param.24) | copy-start | bytes 5505028
  8.0 74.8 %all-gather.5.cloned.1.call-start = ((), (), s32[]{:S(2)}) async-start(), calls=%async_computation.5 | async-start | bytes 7798784 | tf_op jit(solution)/shard_map/all_gather | solution.py:161
  30.5 153.3 %reduce-scatter.3.cloned.1.call-start = ((), (), s32[]{:S(2)}) async-start(), calls=%async_computation.6 | async-start | bytes 8257536 | tf_op jit(solution)/shard_map/reduce_scatter | solution.py:34
  82.8 7.3 %copy-start.8 = (bf16[1792,2048]{1,0:T(8,128)(2,1)S(1)}, bf16[1792,2048]{1,0:T(8,128)(2,1)}, u32[]{:S(2)}) copy-start(bf16[1792,2048]{1,0:T(8,128)(2,1)} %all-gather.5.cloned.1.call-done) | copy-start | bytes 22020100
  82.8 7.3 %copy-start.9 = (bf16[1,2048,448]{1,2,0:T(8,128)(2,1)S(1)}, bf16[1,2048,448]{1,2,0:T(8,128)(2,1)}, u32[]{:S(2)}) copy-start(bf16[1,2048,448]{1,2,0:T(8,128)(2,1)} %param.23) | copy-start | bytes 5505028
  100.0 1.0 copy-start.4
  100.0 2.5 copy-start.3
  100.0 2.7 copy-start.6
  100.0 2.8 copy-start.7
  100.1 83.8 %all-gather.3.cloned.1.call-start = ((), (), s32[]{:S(2)}) async-start(), calls=%async_computation.4 | async-start | bytes 4456448 | tf_op jit(solution)/shard_map/all_gather | solution.py:28
  104.3 94.3 %reduce-scatter.5.cloned.1.call-start = ((), (), s32[]{:S(2)}) async-start(), calls=%async_computation.7 | async-start | bytes 1376256 | tf_op jit(solution)/shard_map/reduce_scatter | solution.py:34
  200.5 152.5 %all-to-all-start.1 = ((bf16[16,7,2048]{2,1,0:T(8,128)(2,1)}), bf16[16,7,2048]{2,1,0:T(8,128)(2,1)S(1)}, u32[]{:S(2)}, u32[]{:S(2)}) async-start(bf16[16,7,2048]{2,1,0:T(8,128)(2,1)} %reshape.467), calls=%async_computation.3 | async-start | bytes 1048576 | tf_op jit(solution)/shard_map/all_to_all | solution.py:168
  211.6 3.4 copy-start.1
  220.6 3.4 copy-start.1
  229.6 3.4 copy-start.1
  238.7 3.4 copy-start.1
  247.7 3.4 copy-start.1
  256.8 3.4 copy-start.1
  265.8 3.4 copy-start.1
  274.8 3.4 copy-start.1
  283.9 3.4 copy-start.1
  292.9 3.4 copy-start.1
  301.9 3.4 copy-start.1
  311.0 3.4 copy-start.1
  320.0 3.4 copy-start.1
  329.0 3.4 copy-start.1
  338.1 3.4 copy-start.1
  347.1 3.4 copy-start.1
  352.4 4.0 %copy-start.2 = (bf16[48,2048]{1,0:T(8,128)(2,1)S(1)}, bf16[48,2048]{1,0:T(8,128)(2,1)}, u32[]{:S(2)}) copy-start(bf16[48,2048]{1,0:T(8,128)(2,1)} %param.19) | copy-start | bytes 589828
  352.4 4.4 %copy-start.5 = (f32[2048]{0:T(1024)S(1)}, f32[2048]{0:T(1024)}, u32[]{:S(2)}) copy-start(f32[2048]{0:T(1024)} %param.25) | copy-start | bytes 24580
Sparse Core Ops, SparseCore 0:
  30.6 52.1 all-gather.4
  100.2 83.5 reduce-scatter.2
  186.3 12.2 reduce-scatter.4
Sparse Core Ops, SparseCore 1:
  104.3 54.8 all-gather.2
where the time goes:
time: 367 us; the launch traced here: 365 us
  waiting for transfers between devices  131 us (36%)
  matrix products  106 us (29%)
  other arithmetic  56.6 us (15%)
  local copies, waits for them, and re-layouts  31.5 us (9%)
  blocking collectives  16.2 us (4%)
  between operations  15.6 us (4%)
  starting transfers between devices  7.61 us (2%)
    reduce_scatter x2, waiting for transfers between devices, sum_by_axis(): subtotal = lax.psum_scatter(subtotal, axis, scatter_dimension=0, tiled=True)  78.2 us
    dot_general x16, matrix products, sweep(): jnp.einsum('hqd,kd->hqk', rotated_queries, key_block, preferred_element_t...  60.3 us
    all_gather x1, waiting for transfers between devices, shards(): lax.all_gather(arrived.reshape(-1, model_width), TP, axis=0, tiled=True)  52.3 us
    reduce_sum x16, other arithmetic, sweep(): row_total = row_total * shrink + jnp.sum(weights, axis=-1)  49.1 us
    dot_general x16, matrix products, sweep(): jnp.einsum('hqk,kd->hdq', weights.astype(jnp.bfloat16), value_block, pref...  28.8 us
    all_to_all x1, blocking collectives, shards(): lax.all_to_all(outgoing.reshape(experts, capacity, model_width), 'ep', sp...  16.2 us
    unnamed x23, local copies, waits for them, and re-layouts  11.2 us
  transfers between devices with their start and end apart: 5, of which 3 were waited for; matrix products, arithmetic and copies ran while one was open for 43% of the time, Pallas kernels for 0%

commit v1 on v0

v1 whole, which is shorter than its diff:
```python
import functools
import math

import jax
import jax.numpy as jnp
import numpy as np
from jax import lax
from jax.experimental import pallas as pl
from jax.experimental.pallas import tpu as pltpu
from jax.sharding import Mesh
from jax.sharding import PartitionSpec as P

KV = 4
GRID_W = 64
TP = ("tp_0", "tp_1")
EP_TP = ("ep", "tp_0", "tp_1")
CAP = 7
HD = 64
HALF = HD // 2
PAIRS = HD // 4
LOG2E = math.log2(math.e)

rope_theta = 10000.0
rms_epsilon = 1e-06
norm_epsilon = 1e-05
residual_scale = 1.4142135623730951

F32 = jnp.float32
BF16 = jnp.bfloat16
VMEM_LIMIT = 56 * 1024 * 1024


def dot(a, b, contract=((1,), (0,))):
    return lax.dot_general(a, b, (contract, ((), ())), preferred_element_type=F32)


def angle_tables(count):
    inverse = (np.float32(rope_theta) ** (-np.arange(PAIRS, dtype=np.float32) / np.float32(PAIRS))).astype(np.float32)
    angles = np.arange(count, dtype=np.float32)[:, None] * inverse
    return np.concatenate([np.cos(angles), np.sin(angles)], axis=1).astype(np.float32)


def spread(row_table, col_table):
    rows = row_table.shape[0]
    width = row_table.shape[1]
    by_row = jnp.broadcast_to(row_table[:, None, :], (rows, GRID_W, width)).reshape(rows * GRID_W, width)
    by_col = jnp.broadcast_to(col_table[None, :, :], (rows, GRID_W, width)).reshape(rows * GRID_W, width)
    cosines = jnp.concatenate([by_row[:, :PAIRS], by_col[:, :PAIRS]], axis=1)
    sines = jnp.concatenate([by_row[:, PAIRS:], by_col[:, PAIRS:]], axis=1)
    return cosines, sines


def rotate(heads, gain, cosines, sines):
    squares = jnp.mean(heads * heads, axis=-1, keepdims=True)
    heads = heads * lax.rsqrt(squares + rms_epsilon) * gain
    a = heads[:, :HALF]
    b = heads[:, HALF:]
    return jnp.concatenate([a * cosines - b * sines, b * cosines + a * sines], axis=1)


def key_kernel(place, keys, values, gain, row_table, col_table, out):
    low = place[1] == 0
    k = jnp.where(low, keys[:, :HD], keys[:, HD:]).astype(F32)
    v = jnp.where(low, values[:, :HD], values[:, HD:])
    cosines, sines = spread(row_table[...], col_table[...])
    out[...] = jnp.concatenate([rotate(k, gain[...], cosines, sines).astype(BF16), v], axis=1)


def query_kernel(place, queries, gain, row_table, col_table, out):
    cosines, sines = spread(row_table[...], col_table[...])
    q = rotate(queries[...].astype(F32), gain[...], cosines, sines).astype(BF16)
    scaled = q.astype(F32) * F32(LOG2E * HD**-0.5)
    high = scaled.astype(BF16)
    out[...] = jnp.concatenate([high, (scaled - high.astype(F32)).astype(BF16)], axis=1)


def attend_kernel(q_ref, near_ref, far_ref, out_ref, kk_ref, v1_ref, top_ref, acc_ref, *, block_q, steps):
    step = pl.program_id(0)
    block_k = kk_ref.shape[0]

    def stage(kv):
        lane = lax.broadcasted_iota(jnp.int32, kv.shape, 1)
        kk_ref[...] = jnp.concatenate([kv[:, :HD], kv[:, :HD]], axis=1)
        v1_ref[...] = jnp.where(lane < HD, jnp.ones_like(kv), kv)

    @pl.when(step < steps)
    def _():
        stage(near_ref[...])

    @pl.when(step >= steps)
    def _():
        stage(far_ref[...])

    count = q_ref.shape[0] // block_q

    @pl.when(step == 0)
    def _():
        for t in range(count):
            rows = pl.ds(t * block_q, block_q)
            s = dot(q_ref[rows, :], kk_ref[:256, :], ((1,), (1,)))
            top_ref[rows, :] = jnp.broadcast_to(jnp.max(s, axis=1, keepdims=True), (block_q, 128))
        acc_ref[...] = jnp.zeros_like(acc_ref)

    def weigh(q, top, k):
        s = dot(q, kk_ref[pl.ds(k * 256, 256), :], ((1,), (1,)))
        p = jnp.exp2(s - jnp.concatenate([top, top], axis=1)).astype(BF16)
        return dot(p, v1_ref[pl.ds(k * 256, 256), :])

    def tile(t, carry):
        rows = pl.ds(pl.multiple_of(t * block_q, block_q), block_q)
        q = q_ref[rows, :]
        top = top_ref[rows, :]
        part = jnp.zeros((block_q, 128), F32)
        for k in range(block_k // 256):
            part = part + weigh(q, top, k)
        over = jnp.max(jnp.where(part[:, :1] < 2.0**100, 0.0, 1.0)) > 0

        @pl.when(jnp.logical_not(over))
        def _():
            acc_ref[rows, :] += part

        @pl.when(over)
        def _():
            def raise_top(k, peak):
                s = dot(q, kk_ref[pl.ds(pl.multiple_of(k * 256, 256), 256), :], ((1,), (1,)))
                return jnp.maximum(peak, jnp.max(s, axis=1, keepdims=True))

            peak = lax.fori_loop(0, block_k // 256, raise_top, jnp.max(top, axis=1, keepdims=True))
            peak = jnp.broadcast_to(peak, (block_q, 128))
            acc_ref[rows, :] = acc_ref[rows, :] * jnp.exp2(top - peak)
            top_ref[rows, :] = peak

            def add(k, carry):
                acc_ref[rows, :] += weigh(q, peak, pl.multiple_of(k, 1))
                return carry

            lax.fori_loop(0, block_k // 256, add, 0)

        return carry

    lax.fori_loop(0, count, tile, 0)

    @pl.when(step == 2 * steps - 1)
    def _():
        a = acc_ref[...]
        out_ref[...] = (a[:, HD:] / a[:, :HD]).astype(BF16)


def attend(q, near, far, block_q=512, block_k=4096):
    rows = q.shape[0]
    steps = near.shape[0] // block_k
    return pl.pallas_call(
        functools.partial(attend_kernel, block_q=block_q, steps=steps),
        grid=(2 * steps,),
        in_specs=[
            pl.BlockSpec((rows, 128), lambda j: (0, 0)),
            pl.BlockSpec((block_k, 128), lambda j: (jnp.minimum(j, steps - 1), 0)),
            pl.BlockSpec((block_k, 128), lambda j: (jnp.maximum(j - steps, 0), 0)),
        ],
        out_specs=pl.BlockSpec((rows, HD), lambda j: (0, 0)),
        out_shape=jax.ShapeDtypeStruct((rows, HD), BF16),
        scratch_shapes=[
            pltpu.VMEM((block_k, 128), BF16),
            pltpu.VMEM((block_k, 128), BF16),
            pltpu.VMEM((rows, 128), F32),
            pltpu.VMEM((rows, 128), F32),
        ],
        compiler_params=pltpu.CompilerParams(vmem_limit_bytes=VMEM_LIMIT),
        cost_estimate=pl.CostEstimate(
            flops=rows * near.shape[0] * 2 * 256 * 4, transcendentals=0, bytes_accessed=near.size * 4
        ),
        name="attend",
    )(q, near, far)


def slots_of(ids, experts):
    tokens = ids.shape[0]
    width = experts * CAP
    slot = lax.broadcasted_iota(jnp.int32, (tokens, width), 1)
    owner = jnp.zeros((tokens, width), jnp.int32)
    for e in range(1, experts):
        owner = owner + (slot >= e * CAP).astype(jnp.int32)
    first = ids[:, 0:1] == owner
    second = ids[:, 1:2] == owner
    named = jnp.where(first | second, 1.0, 0.0)
    row = lax.broadcasted_iota(jnp.int32, (tokens, tokens), 0)
    col = lax.broadcasted_iota(jnp.int32, (tokens, tokens), 1)
    before = dot(jnp.where(col < row, 1.0, 0.0).astype(BF16), named.astype(BF16))
    rank = (slot - owner * CAP).astype(F32)
    taken = (named > 0) & (before == rank)
    return taken, first


def dispatch_kernel(place, ids, rows, out, *, experts):
    taken, ignored = slots_of(ids[...], experts)
    out[...] = dot(jnp.where(taken, 1.0, 0.0).astype(BF16), rows[...], ((0,), (0,))).astype(BF16)


def combine_kernel(place, ids, weights, rows, returned, gain, out, *, experts):
    taken, first = slots_of(ids[...], experts)
    w = weights[...]
    scale = jnp.where(taken, jnp.where(first, w[:, 0:1], w[:, 1:2]), 0.0)
    high = scale.astype(BF16)
    rest = scale - high.astype(F32)
    mid = rest.astype(BF16)
    low = (rest - mid.astype(F32)).astype(BF16)
    back = returned[...]
    mixed = residual_scale * rows[...].astype(F32) + (dot(high, back) + dot(mid, back) + dot(low, back))
    average = jnp.mean(mixed, axis=-1, keepdims=True)
    centered = mixed - average
    variance = jnp.mean(centered * centered, axis=-1, keepdims=True)
    out[...] = (centered * lax.rsqrt(variance + norm_epsilon) * gain[...]).astype(BF16)


def expert_kernel(x_ref, *refs):
    weights, out_ref, bufs, sems = refs[:6], refs[6], refs[7:13], refs[13]
    copies = [pltpu.make_async_copy(w, b, sems.at[i]) for i, (w, b) in enumerate(zip(weights, bufs))]
    for c in copies:
        c.start()
    x = x_ref[...]
    total = None
    for half in range(2):
        gate_b, up_b, down_b = bufs[3 * half : 3 * half + 3]
        copies[3 * half].wait()
        gate = dot(x, gate_b[...])
        copies[3 * half + 1].wait()
        up = dot(x, up_b[...])
        hidden = (gate / (1.0 + jnp.exp(-gate)) * up).astype(BF16)
        copies[3 * half + 2].wait()
        part = dot(hidden, down_b[...])
        total = part if total is None else total + part
    out_ref[...] = total.astype(BF16)


def run_expert(x, weights):
    rows, width = x.shape
    any_spec = pl.BlockSpec(memory_space=pl.ANY)
    return pl.pallas_call(
        expert_kernel,
        in_specs=[pl.BlockSpec((rows, width), lambda: (0, 0))] + [any_spec] * 6,
        out_specs=pl.BlockSpec((rows, width), lambda: (0, 0)),
        out_shape=jax.ShapeDtypeStruct((rows, width), BF16),
        scratch_shapes=[pltpu.VMEM(w.shape, BF16) for w in weights] + [pltpu.SemaphoreType.DMA((6,))],
        compiler_params=pltpu.CompilerParams(vmem_limit_bytes=VMEM_LIMIT),
        cost_estimate=pl.CostEstimate(
            flops=rows * sum(w.size for w in weights) * 2, transcendentals=0, bytes_accessed=2 * sum(w.size for w in weights)
        ),
        name="expert",
    )(x, *weights)


def place_call(body, place, specs, out_block, out_shape, name):
    return pl.pallas_call(
        body,
        grid_spec=pltpu.PrefetchScalarGridSpec(num_scalar_prefetch=1, grid=(1,), in_specs=specs, out_specs=out_block),
        out_shape=out_shape,
        compiler_params=pltpu.CompilerParams(vmem_limit_bytes=VMEM_LIMIT),
        name=name,
    )


def shards(
    queries,
    keys,
    values,
    query_gain,
    key_gain,
    moe_input,
    expert_ids,
    route_weight,
    gate_weight,
    up_weight,
    down_weight,
    output_gain,
):
    seg_rows = queries.shape[0]
    half_rows = seg_rows // 2
    tok_rows, model_width = moe_input.shape
    experts = lax.axis_size("ep")
    column = lax.axis_index(TP)
    ep = lax.axis_index("ep")
    core = lax.axis_index("tp_1")
    key_head = column * KV // lax.axis_size(TP)
    place = jnp.stack([key_head // 2, key_head % 2, ep, core, column]).astype(jnp.int32)

    whole = lambda shape: pl.BlockSpec(shape, lambda i, p: (0, 0))
    own = pl.BlockSpec((tok_rows, 2), lambda i, p: (p[4], 0))
    slots = experts * CAP
    outgoing = place_call(
        functools.partial(dispatch_kernel, experts=experts),
        place,
        [own, whole((tok_rows, model_width))],
        whole((slots, model_width)),
        jax.ShapeDtypeStruct((slots, model_width), BF16),
        "dispatch",
    )(place, expert_ids, moe_input)
    arrived = lax.all_to_all(
        outgoing.reshape(experts, CAP, model_width), "ep", split_axis=0, concat_axis=0, tiled=True
    ).reshape(slots, model_width)

    own_weights = (gate_weight[0], up_weight[0], down_weight[0])
    swap = [(0, 1), (1, 0)]
    other_weights = tuple(lax.ppermute(w, "tp_1", swap) for w in own_weights)

    row_table = jnp.asarray(angle_tables(seg_rows * experts // GRID_W))
    col_table = jnp.asarray(angle_tables(GRID_W))
    kv_grid = half_rows // GRID_W
    kv_rows = pl.BlockSpec((half_rows, 128), lambda i, p: (p[3], p[0]))
    kv_own = place_call(
        key_kernel,
        place,
        [
            kv_rows,
            kv_rows,
            whole((1, HD)),
            pl.BlockSpec((kv_grid, 2 * PAIRS), lambda i, p: (2 * p[2] + p[3], 0)),
            whole((GRID_W, 2 * PAIRS)),
        ],
        whole((half_rows, 2 * HD)),
        jax.ShapeDtypeStruct((half_rows, 2 * HD), BF16),
        "keys",
    )(place, keys, values, key_gain[None], row_table, col_table)
    kv_near = lax.all_gather(kv_own, "ep", axis=0, tiled=True)
    kv_far = lax.ppermute(kv_near, "tp_1", swap)
    q = place_call(
        query_kernel,
        place,
        [
            whole((seg_rows, HD)),
            whole((1, HD)),
            pl.BlockSpec((seg_rows // GRID_W, 2 * PAIRS), lambda i, p: (p[2], 0)),
            whole((GRID_W, 2 * PAIRS)),
        ],
        whole((seg_rows, 2 * HD)),
        jax.ShapeDtypeStruct((seg_rows, 2 * HD), BF16),
        "queries",
    )(place, queries, query_gain[None], row_table, col_table)

    gathered = lax.all_gather(arrived, "tp_0", axis=0, tiled=True)
    partial = run_expert(gathered, own_weights + other_weights)
    expert_out = lax.psum_scatter(partial, "tp_0", scatter_dimension=0, tiled=True)
    attended = attend(q, kv_near, kv_far)
    returned = lax.all_to_all(
        expert_out.reshape(experts, CAP, model_width), "ep", split_axis=0, concat_axis=0, tiled=True
    ).reshape(slots, model_width)
    moe_output = place_call(
        functools.partial(combine_kernel, experts=experts),
        place,
        [own, own, whole((tok_rows, model_width)), whole((slots, model_width)), whole((1, model_width))],
        whole((tok_rows, model_width)),
        jax.ShapeDtypeStruct((tok_rows, model_width), BF16),
        "combine",
    )(place, expert_ids, route_weight, moe_input, returned, output_gain[None])
    return (attended, moe_output)


def solution(mesh):
    split = Mesh(mesh.devices.reshape(mesh.shape["ep"], 8, 2), ("ep", "tp_0", "tp_1"))
    return jax.shard_map(
        shards,
        mesh=split,
        in_specs=(
            P("ep", TP),
            P("ep", None),
            P("ep", None),
            P(),
            P(),
            P(EP_TP, None),
            P("ep", None),
            P("ep", None),
            P("ep", None, TP),
            P("ep", None, TP),
            P("ep", TP, None),
            P(),
        ),
        out_specs=(P("ep", TP), P(EP_TP, None)),
        check_vma=False,
    )
```

time: 367 us -> 330 us (0.90)
  Pallas kernels: 0 us -> 151 us
  matrix products: 106 us -> 0 us
  other arithmetic: 56.6 us -> 0 us
  waiting for transfers between devices: 131 us -> 114 us
  local copies, waits for them, and re-layouts: 31.5 us -> 26 us
    pallas_call x0 -> x6, Pallas kernels: none -> 151 us  [the longest x1 121 us: attend(): pl.pallas_call(functools.partial(attend_kernel, block_q=block_q, steps=st...]
    dot_general x35 -> x0, matrix products: 106 us -> none  [the longest x16 60.3 us: sweep(): jnp.einsum('hqd,kd->hqk', rotated_queries, key_block, preferred_element_t...]
    reduce_sum x22 -> x0, other arithmetic: 51.8 us -> none  [the longest x16 49.1 us: sweep(): row_total = row_total * shrink + jnp.sum(weights, axis=-1)]
    reduce_scatter x2 -> x1, waiting for transfers between devices: 78.2 us -> 48.2 us  [shards(): lax.psum_scatter(partial, 'tp_0', scatter_dimension=0, tiled=True)]
    all_gather x2, waiting for transfers between devices: 52.3 us -> 65.9 us  [the longest x1 33.6 us: shards(): gathered = lax.all_gather(arrived, 'tp_0', axis=0, tiled=True)]
    ppermute x0 -> x2, local copies, waits for them, and re-layouts: none -> 7.62 us  [shards(): other_weights = tuple((lax.ppermute(w, 'tp_1', swap) for w in own_weights))]
    while x48 -> x0, local copies, waits for them, and re-layouts: 5.37 us -> none
    split x1 -> x0, local copies, waits for them, and re-layouts: 4.65 us -> none  [side_by_side(): jnp.split(lax.all_gather(both, axis, axis=dim, tiled=True), ends, axis=al...]
  transfers between devices with their start and end apart: 5 -> 8, of which waited for: 3 -> 3; matrix products, arithmetic and copies ran while one was open for 43% -> 6% of each run, Pallas kernels for 0% -> 44%
where the time goes in v1:
time: 330 us
  Pallas kernels  151 us (46%)
  waiting for transfers between devices  114 us (35%)
  local copies, waits for them, and re-layouts  26 us (8%)
  blocking collectives  16.3 us (5%)
  between operations  13.9 us (4%)
  starting transfers between devices  8.09 us (2%)
    pallas_call x1, Pallas kernels, attend(): pl.pallas_call(functools.partial(attend_kernel, block_q=block_q, steps=st...  121 us
    reduce_scatter x1, waiting for transfers between devices, shards(): lax.psum_scatter(partial, 'tp_0', scatter_dimension=0, tiled=True)  48.2 us
    all_gather x1, waiting for transfers between devices, shards(): gathered = lax.all_gather(arrived, 'tp_0', axis=0, tiled=True)  33.6 us
    all_gather x1, waiting for transfers between devices, shards(): kv_near = lax.all_gather(kv_own, 'ep', axis=0, tiled=True)  32.3 us
    pallas_call x1, Pallas kernels, run_expert(): pl.pallas_call(expert_kernel, in_specs=[pl.BlockSpec((rows, width), lambd...  18.3 us
    all_to_all x1, blocking collectives, shards(): lax.all_to_all(outgoing.reshape(experts, CAP, model_width), 'ep', split_a...  16.3 us
    unnamed x14, local copies, waits for them, and re-layouts  12.8 us
    ppermute x2, local copies, waits for them, and re-layouts, shards(): other_weights = tuple((lax.ppermute(w, 'tp_1', swap) for w in own_weights))  7.62 us
  transfers between devices with their start and end apart: 8, of which 3 were waited for; matrix products, arithmetic and copies ran while one was open for 6% of the time, Pallas kernels for 44%

profile of v1, /device:TPU:4, one launch (start us, length us, event | category | flops | bytes accessed | tf_op | source)
XLA Modules:
  0.0 329.5 jit_solution(5729029034274847251)
XLA Ops:
  7.2 0.0 all-gather.5.cloned.1.call-start
  7.3 1.6 copy.38.ids
  8.9 0.7 stack.23.place
  9.5 2.9 dispatch.1
  12.4 1.2 reshape.16
  13.6 0.0 copy-start
  13.6 16.3 %all_to_all.10 = bf16[16,7,2048]{2,1,0:T(8,128)(2,1)S(1)} all-to-all(bf16[16,7,2048]{2,1,0:T(8,128)(2,1)S(1)} %reshape.16), channel_id=1, replica_groups=mesh['ep'=16,'tp_0'=8,'tp_1'=2] {'ep'}, dimensions={0} | all-to-all | bytes 917504 | tf_op jit(solution)/shard_map/all_to_all | solution.py:297
  29.9 0.9 reshape.17
  30.8 0.0 all-gather.5.cloned.1.call-update
  30.8 0.0 all-gather.3.cloned.1.call-start
  30.9 2.9 keys.2
  33.8 0.0 all-gather.3.cloned.1.call-update
  33.9 0.0 reduce-scatter.2.cloned.1.call-start
  33.9 0.0 copy-done
  33.9 0.1 collective-permute-start.1
  34.0 0.5 collective-permute-start.2
  34.5 0.1 collective-permute-start.3
  34.6 2.4 copy.32
  37.0 3.8 %copy.33 = bf16[1,2048,448]{2,1,0:T(8,128)(2,1)} copy(bf16[1,2048,448]{1,2,0:T(8,128)(2,1)} %param.23) | data formatting | bytes 3670016 | tf_op args[9]
  40.8 0.0 collective-permute-done.1
  40.8 3.8 %copy.36.refs_3_ = bf16[2048,448]{1,0:T(8,128)(2,1)} copy(bf16[2048,448]{0,1:T(8,128)(2,1)} %collective-permute-done.1) | data formatting | bytes 3670016 | tf_op jit(solution)/shard_map/ppermute | solution.py:303
  44.7 0.0 collective-permute-done.2
  44.7 3.8 %copy.37.refs_4_ = bf16[2048,448]{1,0:T(8,128)(2,1)} copy(bf16[2048,448]{0,1:T(8,128)(2,1)} %collective-permute-done.2) | data formatting | bytes 3670016 | tf_op jit(solution)/shard_map/ppermute | solution.py:303
  48.5 0.0 collective-permute-done.3.refs_5_
  48.5 33.6 %all-gather.5.cloned.1.call-done.x_ref = bf16[896,2048]{1,0:T(8,128)(2,1)} async-done(((bf16[112,2048]{1,0:T(8,128)(2,1)}), bf16[896,2048]{1,0:T(8,128)(2,1)}) %all-gather.5.cloned.1.call-update) | async-done | bytes 3670032 | tf_op jit(solution)/shard_map/all_gather | solution.py:339
  82.1 18.3 %expert.1 = bf16[896,2048]{1,0:T(8,128)(2,1)} custom-call(bf16[896,2048]{1,0:T(8,128)(2,1)} %all-gather.5.cloned.1.call-done.x_ref, bf16[2048,448]{1,0:T(8,128)(2,1)} %bitcast.13, bf16[2048,448]{1,0:T(8,128)(2,1)} %bitcast.14, bf16[448,2048]{1,0:T(8,128)(2,1)} %bitcast.21, bf16[2048,448]{1,0:T(8,128)(2,1)} %copy.36.refs_3_, bf16[2048,448]{1,0:T(8,128)(2,1)} %copy.37.refs_4_, ...), custom_call_target="tpu_custom_call" | custom-call | flops 9865003008 | bytes 11010048 | tf_op jit(solution)/shard_map/expert/pallas_call | solution.py:238
  100.4 0.0 copy-start.2
  100.4 0.0 copy-start.1
  100.4 0.0 reduce-scatter.2.cloned.1.call-update
  100.4 32.3 %all-gather.3.cloned.1.call-done.near_ref = bf16[8192,128]{1,0:T(8,128)(2,1)} async-done(((bf16[512,128]{1,0:T(8,128)(2,1)}), bf16[8192,128]{1,0:T(8,128)(2,1)}) %all-gather.3.cloned.1.call-update) | async-done | bytes 2097168 | tf_op jit(solution)/shard_map/all_gather | solution.py:323
  132.7 0.0 collective-permute-start
  132.7 0.0 copy-done.2
  132.7 1.0 copy.39.weights
  133.7 0.0 copy-done.1
  133.7 0.8 copy.30.queries
  134.5 3.3 queries.2.q_ref
  137.8 48.2 %reduce-scatter.2.cloned.1.call-done = bf16[112,2048]{1,0:T(8,128)(2,1)} async-done(((bf16[896,2048]{1,0:T(8,128)(2,1)}), bf16[112,2048]{1,0:T(8,128)(2,1)}) %reduce-scatter.2.cloned.1.call-update) | async-done | bytes 458768 | tf_op jit(solution)/shard_map/reduce_scatter | solution.py:341
  186.0 2.0 reshape.18
  188.0 7.3 %all-to-all-start.1 = ((bf16[16,7,2048]{2,1,0:T(8,128)(2,1)}), bf16[16,7,2048]{2,1,0:T(8,128)(2,1)S(1)}, u32[]{:S(2)}, u32[]{:S(2)}) async-start(bf16[16,7,2048]{2,1,0:T(8,128)(2,1)} %reshape.18), calls=%async_computation.2 | async-start | bytes 1048576 | tf_op jit(solution)/shard_map/all_to_all | solution.py:343
  195.3 0.0 collective-permute-done.far_ref
  195.3 0.0 copy-start.3
  195.3 1.3 copy-done.3
  196.6 120.5 %attend.1 = bf16[1024,64]{1,0:T(8,128)(2,1)} custom-call(bf16[1024,128]{1,0:T(8,128)(2,1)} %queries.2.q_ref, bf16[8192,128]{1,0:T(8,128)(2,1)} %all-gather.3.cloned.1.call-done.near_ref, bf16[8192,128]{1,0:T(8,128)(2,1)} %copy-done.3), custom_call_target="tpu_custom_call" | custom-call | flops 17179869184 | bytes 4194304 | tf_op jit(solution)/shard_map/attend/pallas_call | solution.py:152
  317.1 1.7 copy.40
  318.9 0.0 all-to-all-done.1
  318.9 0.9 reshape.19.returned
  319.8 3.2 combine.1
Async XLA Ops:
  7.2 74.9 %all-gather.5.cloned.1.call-start = ((), (), s32[]{:S(2)}) async-start(), calls=%async_computation.4 | async-start | bytes 4128768 | tf_op jit(solution)/shard_map/all_gather | solution.py:339
  13.6 20.3 %copy-start = (bf16[1,2048,448]{1,2,0:T(8,128)(2,1)S(1)}, bf16[1,2048,448]{1,2,0:T(8,128)(2,1)}, u32[]{:S(2)}) copy-start(bf16[1,2048,448]{1,2,0:T(8,128)(2,1)} %param.22) | copy-start | bytes 5505028
  30.8 101.9 %all-gather.3.cloned.1.call-start = ((), (), s32[]{:S(2)}) async-start(), calls=%async_computation.3 | async-start | bytes 2228224 | tf_op jit(solution)/shard_map/all_gather | solution.py:323
  33.9 152.2 %reduce-scatter.2.cloned.1.call-start = ((), (), s32[]{:S(2)}) async-start(), calls=%async_computation.5 | async-start | bytes 4128768 | tf_op jit(solution)/shard_map/reduce_scatter | solution.py:341
  33.9 6.9 %collective-permute-start.1 = (bf16[2048,448]{0,1:T(8,128)(2,1)S(1)}, bf16[2048,448]{0,1:T(8,128)(2,1)}, u32[]{:S(2)}, u32[]{:S(2)}) collective-permute-start(bf16[2048,448]{0,1:T(8,128)(2,1)S(1)} %bitcast.15), channel_id=1, source_target_pairs={{0,1},{1,0},{2,3},{3,2},{4,5},{5,4},{6,7},{7,6},{8,9},{9,8},{10,11... | collective-permute-start | bytes 5505032 | tf_op jit(solution)/shard_map/ppermute | solution.py:303
  34.0 10.7 %collective-permute-start.2 = (bf16[2048,448]{0,1:T(8,128)(2,1)}, bf16[2048,448]{0,1:T(8,128)(2,1)}, u32[]{:S(2)}, u32[]{:S(2)}) collective-permute-start(bf16[2048,448]{0,1:T(8,128)(2,1)} %bitcast.16), channel_id=1, source_target_pairs={{0,1},{1,0},{2,3},{3,2},{4,5},{5,4},{6,7},{7,6},{8,9},{9,8},{10,11... | collective-permute-start | bytes 5505032 | tf_op jit(solution)/shard_map/ppermute | solution.py:303
  34.5 14.0 %collective-permute-start.3 = (bf16[448,2048]{1,0:T(8,128)(2,1)}, bf16[448,2048]{1,0:T(8,128)(2,1)}, u32[]{:S(2)}, u32[]{:S(2)}) collective-permute-start(bf16[448,2048]{1,0:T(8,128)(2,1)} %bitcast.20), channel_id=1, source_target_pairs={{0,1},{1,0},{2,3},{3,2},{4,5},{5,4},{6,7},{7,6},{8,9},{9,8},{10,11... | collective-permute-start | bytes 5505032 | tf_op jit(solution)/shard_map/ppermute | solution.py:303
  100.4 32.4 %copy-start.2 = (f32[768,2]{0,1:T(2,128)S(1)}, f32[768,2]{0,1:T(2,128)}, u32[]{:S(2)}) copy-start(f32[768,2]{0,1:T(2,128)} %param.21) | copy-start | bytes 18436
  100.4 33.3 %copy-start.1 = (bf16[1024,64]{0,1:T(8,128)(2,1)S(1)}, bf16[1024,64]{0,1:T(8,128)(2,1)}, u32[]{:S(2)}) copy-start(bf16[1024,64]{0,1:T(8,128)(2,1)} %param.14) | copy-start | bytes 393220
  132.7 62.5 %collective-permute-start = (bf16[8192,128]{1,0:T(8,128)(2,1)}, bf16[8192,128]{1,0:T(8,128)(2,1)S(1)}, u32[]{:S(2)}, u32[]{:S(2)}) collective-permute-start(bf16[8192,128]{1,0:T(8,128)(2,1)} %all-gather.3.cloned.1.call-done.near_ref), channel_id=1, source_target_pairs={{0,1},{1,0},{2,3},{3,2},{4,5},{5,4},{6,7},{7,6},{8,9},{9,8},{10,11... | collective-permute-start | bytes 6291464 | tf_op jit(solution)/shard_map/ppermute | solution.py:324
  188.0 130.9 %all-to-all-start.1 = ((bf16[16,7,2048]{2,1,0:T(8,128)(2,1)}), bf16[16,7,2048]{2,1,0:T(8,128)(2,1)S(1)}, u32[]{:S(2)}, u32[]{:S(2)}) async-start(bf16[16,7,2048]{2,1,0:T(8,128)(2,1)} %reshape.18), calls=%async_computation.2 | async-start | bytes 1048576 | tf_op jit(solution)/shard_map/all_to_all | solution.py:343
  195.3 1.4 copy-start.3
Sparse Core Ops, SparseCore 0:
  31.0 51.0 all-gather.4
  85.1 47.5 all-gather.2
  135.3 50.6 reduce-scatter.1
